TPU v7x, 256 devices: a whole 4x4x8 slice. The times are simulated.
256 devices in a mesh: kv: 32 (over z, y), tp: 8 (over x, core).
Axes of the slice: x: 4, y: 4, z: 8, core: 2. Of those that a mesh axis runs over, the one named last changes fastest.
Arguments:
- stream: bfloat16 [24, 4096], P(None, ('kv', 'tp')), may hold values from -50 to 50
- attention_gain: float32 [4096], P(('kv', 'tp')), may hold values from 0.1 to 1.9
- query_down: bfloat16 [4096, 1536], P(('kv', 'tp')), may hold values from -0.09375 to 0.09375
- latent_down: bfloat16 [4096, 512], P(('kv', 'tp')), may hold values from -0.09375 to 0.09375
- rotary_down: bfloat16 [4096, 64], P(('kv', 'tp')), may hold values from -0.1875 to 0.1875
- query_gain: float32 [1536], replicated, may hold values from 0.1 to 1.9
- latent_gain: float32 [512], replicated, may hold values from 0.1 to 1.9
- query_content: bfloat16 [1536, 2048], P(None, 'tp'), may hold values from -0.15625 to 0.15625
- query_rotary: bfloat16 [1536, 1024], P(None, 'tp'), may hold values from -0.15625 to 0.15625
- key_absorb: bfloat16 [16, 128, 512], P('tp'), may hold values from -0.5 to 0.5
- value_absorb: bfloat16 [16, 512, 128], P('tp'), may hold values from -0.25 to 0.25
- latent_cache: bfloat16 [24, 8192, 512], P(None, 'kv'), may hold values from -1200 to 1200
- rotary_cache: bfloat16 [24, 8192, 64], P(None, 'kv'), may hold values from -5 to 5
- head_gain: float32 [2048], P('tp'), may hold values from 0.1 to 1.9
- output_weight: bfloat16 [2048, 4096], P('tp', 'kv'), may hold values from -0.125 to 0.125
- mixer_gain: float32 [4096], P('kv'), may hold values from 0.1 to 1.9
- gate_weight: bfloat16 [4096, 11264], P('kv', 'tp'), may hold values from -0.09375 to 0.09375
- up_weight: bfloat16 [4096, 11264], P('kv', 'tp'), may hold values from -0.09375 to 0.09375
- down_weight: bfloat16 [11264, 4096], P('tp', 'kv'), may hold values from -0.0546875 to 0.0546875
Outputs:
- stream_out: bfloat16 [24, 4096], P(None, ('kv', 'tp'))
All inputs are finite; a program needn't handle non-finite values.
Results may differ from a plain program's by a relative error of at most 0.018.
Values may be sent and summed in bfloat16 or wider, within the bound.
No kernel may reach another device: no remote copies, remote signals or barrier semaphores. Data moves between devices by JAX's collectives and lax.ppermute only.
A program may use at most 64 MiB of HBM per device.

v0:
```python
import jax
import jax.numpy as jnp
from jax import lax
from jax.sharding import Mesh
from jax.sharding import PartitionSpec as P

KV = ("kv_0", "kv_1")
TP = ("tp_0", "tp_1")
KV_TP = ("kv_0", "kv_1", "tp_0", "tp_1")


epsilon = 1e-06
rope_base = 10000.0


def copy_for_each(x, axis):
    copies = jnp.broadcast_to(x, (lax.axis_size(axis), *x.shape))
    return lax.all_to_all(copies, axis, split_axis=0, concat_axis=0, tiled=True)


def joined_along(parts, dim):
    shape = list(parts.shape[1:])
    shape[dim] *= parts.shape[0]
    return jnp.moveaxis(parts, 0, dim).reshape(shape)


def gather_directly(x, axis, dim):
    parts = copy_for_each(x, axis)
    return joined_along(parts, dim)


def filled_up(lines, count):
    spare = -len(lines) % count
    return jnp.pad(lines, [(0, spare)] + [(0, 0)] * (lines.ndim - 1))


def whole_of(x, axes, dim):
    far, near = axes
    first = copy_for_each(x, far)
    parts = jnp.swapaxes(copy_for_each(first, near), 0, 1)
    return joined_along(parts.reshape(-1, *x.shape), dim)


def cut_along(x, dim, count):
    before, after = (x.shape[:dim], x.shape[dim + 1 :])
    return jnp.moveaxis(x.reshape(*before, count, -1, *after), dim, 0)


def sent_and_summed(x, axis, dim):
    count = lax.axis_size(axis)
    parts = lax.all_to_all(cut_along(x, dim, count), axis, 0, 0, tiled=True)
    return jnp.sum(parts, axis=0)


def sum_in_two_steps(x, axes, dim):
    far, near = axes
    parts = cut_along(x, dim, lax.axis_size(far))
    nearer = sent_and_summed(parts, near, dim + 1)
    arrived = lax.all_to_all(nearer, far, split_axis=0, concat_axis=0, tiled=True)
    return arrived.sum(axis=0)


def nested_sum(x, axes):
    padded = filled_up(x, lax.axis_size(axes[0]) * lax.axis_size(axes[1]))
    whole = whole_of(sum_in_two_steps(padded, axes, 0), axes, 0)
    return lax.slice_in_dim(whole, 0, len(x)).reshape(x.shape)


def packed_total(arrays, axis):
    flat, at, done = (jnp.concatenate([a.reshape(-1) for a in arrays]), 0, [])
    subtotal = nested_sum(flat, axis)
    for a in arrays:
        done.append(subtotal[at : at + a.size].reshape(a.shape))
        at += a.size
    return tuple(done)


def side_by_side(arrays, axis, dim, along):
    widths = [a.shape[along] for a in arrays]
    both = jnp.concatenate(arrays, axis=along)
    whole = lax.all_gather(both, axis, axis=dim, tiled=True)
    return tuple(jnp.split(whole, [sum(widths[:k]) for k in range(1, len(widths))], axis=along))


def of_everyone(x, axis):
    return copy_for_each(x, axis).sum(axis=0)


def over_copies(x, axis):
    return copy_for_each(x, axis).astype(jnp.float32).sum(axis=0)


def sum_at_owner(x, axis, dim):
    parts = cut_along(x, dim, lax.axis_size(axis))
    arrived = lax.all_to_all(parts, axis, split_axis=0, concat_axis=0, tiled=True)
    return arrived.astype(jnp.float32).sum(axis=0)


def nested_sum_2(x, axes):
    lines = x.reshape(-1)
    own = sum_at_owner(filled_up(lines, lax.axis_size(axes)), axes, 0)
    whole = gather_directly(own.astype(jnp.bfloat16), axes, 0)
    return whole[: len(lines)].reshape(x.shape).astype(jnp.float32)


def rotate(values, position):
    half = values.shape[-1] // 2
    freqs = rope_base ** (-jnp.arange(half, dtype=jnp.float32) * 2.0 / values.shape[-1])
    angle = position * freqs
    cosine = jnp.cos(angle)
    sine = jnp.sin(angle)
    first = values[..., :half]
    second = values[..., half:]
    return jnp.concatenate(
        [first * cosine - second * sine, second * cosine + first * sine], axis=-1
    )


def inv_rms(values):
    return lax.rsqrt(jnp.mean(values * values, axis=-1) + epsilon)


def sum_squares(values):
    return jnp.sum(values * values, axis=-1)


def matmul(left, right):
    return jnp.dot(left, right, preferred_element_type=jnp.float32)


def local(
    stream,
    attention_gain,
    query_down,
    latent_down,
    rotary_down,
    query_gain,
    latent_gain,
    query_content,
    query_rotary,
    key_absorb,
    value_absorb,
    latent_cache,
    rotary_cache,
    head_gain,
    output_weight,
    mixer_gain,
    gate_weight,
    up_weight,
    down_weight,
):
    kv_count = lax.axis_size(KV)
    tp_count = lax.axis_size(TP)
    batch_rows = stream.shape[0]
    model_width = stream.shape[1] * kv_count * tp_count
    position = jnp.float32(latent_cache.shape[1] * kv_count)
    stream_block = gather_directly(stream, TP, 1)
    stream_f = stream.astype(jnp.float32)
    first_scaled = (stream_f * attention_gain).astype(jnp.bfloat16)
    query_sum, latent_sum, rotary_sum, square_sum = packed_total(
        (
            matmul(first_scaled, query_down),
            matmul(first_scaled, latent_down),
            matmul(first_scaled, rotary_down),
            sum_squares(stream_f),
        ),
        (("kv_0", "kv_1"), ("tp_0", "tp_1")),
    )
    first_scale = lax.rsqrt(square_sum / model_width + epsilon)[:, None]
    query_low = first_scale * query_sum
    latent_new = first_scale * latent_sum
    rotary_new = first_scale * rotary_sum
    query_normed = (query_low * inv_rms(query_low)[:, None] * query_gain).astype(jnp.bfloat16)
    latent_row = (latent_new * inv_rms(latent_new)[:, None] * latent_gain).astype(jnp.bfloat16)
    rotary_row = rotate(rotary_new, position).astype(jnp.bfloat16)
    heads_here = key_absorb.shape[0]
    query_plain = matmul(query_normed, query_content).astype(jnp.bfloat16)
    query_plain = query_plain.reshape(batch_rows, heads_here, key_absorb.shape[1])
    query_turned = matmul(query_normed, query_rotary).reshape(
        batch_rows, heads_here, rotary_cache.shape[2]
    )
    query_turned = rotate(query_turned, position).astype(jnp.bfloat16)
    query_latent = jnp.einsum(
        "bhn,hnc->bhc", query_plain, key_absorb, preferred_element_type=jnp.float32
    ).astype(jnp.bfloat16)
    scale = (key_absorb.shape[1] + rotary_cache.shape[2]) ** (-0.5)
    scores = (
        jnp.einsum("bhc,bpc->bhp", query_latent, latent_cache, preferred_element_type=jnp.float32)
        + jnp.einsum("bhr,bpr->bhp", query_turned, rotary_cache, preferred_element_type=jnp.float32)
    ) * scale
    maxima = jnp.max(scores, axis=-1)
    expo = jnp.exp(scores - maxima[..., None])
    totals = jnp.sum(expo, axis=-1)
    weighted = jnp.einsum(
        "bhp,bpc->bhc", expo.astype(jnp.bfloat16), latent_cache, preferred_element_type=jnp.float32
    ).astype(jnp.bfloat16)
    all_maxima, all_totals = side_by_side((maxima[None], totals[None]), KV, 0, 1)
    own_score = (
        jnp.sum(
            query_latent.astype(jnp.float32) * latent_row.astype(jnp.float32)[:, None, :], axis=-1
        )
        + jnp.sum(
            query_turned.astype(jnp.float32) * rotary_row.astype(jnp.float32)[:, None, :], axis=-1
        )
    ) * scale
    largest = jnp.maximum(jnp.max(all_maxima, axis=0), own_score)
    factors = jnp.exp(all_maxima - largest[None])
    own_weight = jnp.exp(own_score - largest)
    denominator = jnp.sum(factors * all_totals, axis=0) + own_weight
    pieces = lax.all_to_all(weighted[None], KV, split_axis=3, concat_axis=0, tiled=True)
    share = pieces.shape[3]
    own_cols = lax.dynamic_slice_in_dim(latent_row, lax.axis_index(KV) * share, share, 1)
    merged = jnp.sum(factors[..., None] * pieces.astype(jnp.float32), axis=0)
    merged = merged + own_weight[..., None] * own_cols.astype(jnp.float32)[:, None, :]
    columns = (merged / denominator[..., None]).astype(jnp.bfloat16)
    latent_mix = gather_directly(columns, KV, 2)
    head_values = jnp.einsum(
        "bhc,hcv->bhv", latent_mix, value_absorb, preferred_element_type=jnp.float32
    ).astype(jnp.bfloat16)
    head_f = head_values.reshape(batch_rows, heads_here * value_absorb.shape[2]).astype(jnp.float32)
    head_square = of_everyone(sum_squares(head_f), TP)
    head_scale = lax.rsqrt(head_square / (head_f.shape[1] * tp_count) + epsilon)[:, None]
    head_scaled = (head_f * head_gain).astype(jnp.bfloat16)
    attended = over_copies(matmul(head_scaled, output_weight).astype(jnp.bfloat16), TP).astype(
        jnp.float32
    )
    middle = (stream_block.astype(jnp.float32) + head_scale * attended).astype(jnp.bfloat16)
    middle_f = middle.astype(jnp.float32)
    second_scaled = (middle_f * mixer_gain).astype(jnp.bfloat16)
    gate_part = matmul(second_scaled, gate_weight)
    up_part = matmul(second_scaled, up_weight)
    gate_total, up_total, middle_square = (
        nested_sum_2(gate_part.astype(jnp.bfloat16), KV),
        nested_sum_2(up_part.astype(jnp.bfloat16), KV),
        nested_sum_2(sum_squares(middle_f).astype(jnp.bfloat16), KV),
    )
    second_scale = lax.rsqrt(middle_square / model_width + epsilon)[:, None]
    hidden = (jax.nn.silu(second_scale * gate_total) * (second_scale * up_total)).astype(
        jnp.bfloat16
    )
    mixed = sum_at_owner(matmul(hidden, down_weight).astype(jnp.bfloat16), TP, 1)
    share_width = mixed.shape[1]
    own_middle = lax.dynamic_slice_in_dim(
        middle_f, lax.axis_index(TP) * share_width, share_width, 1
    )
    return (own_middle + mixed).astype(jnp.bfloat16)


def solution(mesh):
    finer = Mesh(mesh.devices.reshape(8, 4, 4, 2), ("kv_0", "kv_1", "tp_0", "tp_1"))
    return jax.shard_map(
        local,
        mesh=finer,
        in_specs=(
            P(None, KV_TP),
            P(KV_TP),
            P(KV_TP, None),
            P(KV_TP, None),
            P(KV_TP, None),
            P(),
            P(),
            P(None, TP),
            P(None, TP),
            P(TP, None, None),
            P(TP, None, None),
            P(None, KV, None),
            P(None, KV, None),
            P(TP),
            P(TP, KV),
            P(KV),
            P(KV, TP),
            P(KV, TP),
            P(TP, KV),
        ),
        out_specs=P(None, KV_TP),
        check_vma=False,
    )
```

profile of v0, /device:TPU:1, one launch (start us, length us, event | category | flops | bytes accessed | tf_op | source)
XLA Modules:
  0.0 288.2 jit_solution(4064149729000868377)
XLA Ops:
  2.8 1.1 fusion.37
  4.4 12.1 %all_to_all.110 = f32[8,32,199]{2,1,0:T(8,128)S(1)} all-to-all(f32[8,32,199]{2,1,0:T(8,128)S(1)} %copy.144), channel_id=1, replica_groups=mesh['kv_0'=8,'kv_1'=4,'tp_0'=4,'tp_1'=2] {'tp_0','tp_1'}, dimensions={0} | all-to-all | bytes 407552 | tf_op jit(solution)/shard_map/all_to_all | solution.py:51
  16.6 19.7 %all_to_all.111 = f32[32,1,199]{2,1,0:T(1,128)S(1)} all-to-all(f32[32,1,199]{2,1,0:T(1,128)S(1)} %all_to_all.73), channel_id=1, replica_groups=mesh['kv_0'=8,'kv_1'=4,'tp_0'=4,'tp_1'=2] {'kv_0','kv_1'}, dimensions={0} | all-to-all | bytes 50944 | tf_op jit(solution)/shard_map/all_to_all | solution.py:59
  37.0 3.9 %all-to-all-start.3 = ((f32[32,1,199]{2,1,0:T(1,128)}), f32[32,1,199]{2,1,0:T(1,128)S(1)}, u32[]{:S(2)}, u32[]{:S(2)}) async-start(f32[32,1,199]{2,1,0:T(1,128)} %broadcast_in_dim.25), calls=%async_computation.3 | async-start | bytes 65536 | tf_op jit(solution)/shard_map/all_to_all | solution.py:18
  42.2 7.2 %all-to-all-done.3 = f32[32,1,199]{2,1,0:T(1,128)S(1)} async-done(((f32[32,1,199]{2,1,0:T(1,128)}), f32[32,1,199]{2,1,0:T(1,128)S(1)}, u32[]{:S(2)}, u32[]{:S(2)}) %all-to-all-start.3) | async-done | bytes 25504 | tf_op jit(solution)/shard_map/all_to_all | solution.py:18
  49.5 6.8 %all-to-all-start = ((bf16[8,2,192]{2,1,0:T(2,128)(2,1)}), bf16[8,2,192]{2,1,0:T(2,128)(2,1)S(1)}, u32[]{:S(2)}, u32[]{:S(2)}) async-start(bf16[8,2,192]{2,1,0:T(2,128)(2,1)} %reshape.275), calls=%async_computation | async-start | bytes 16384 | tf_op jit(solution)/shard_map/all_to_all | solution.py:18
  56.2 4.6 %all-to-all-done = bf16[8,2,192]{2,1,0:T(2,128)(2,1)S(1)} async-done(((bf16[8,2,192]{2,1,0:T(2,128)(2,1)}), bf16[8,2,192]{2,1,0:T(2,128)(2,1)S(1)}, u32[]{:S(2)}, u32[]{:S(2)}) %all-to-all-start) | async-done | bytes 6176 | tf_op jit(solution)/shard_map/all_to_all | solution.py:18
  61.6 4.0 %all-to-all-start.4 = ((f32[8,32,199]{2,1,0:T(8,128)}), f32[8,32,199]{2,1,0:T(8,128)S(1)}, u32[]{:S(2)}, u32[]{:S(2)}) async-start(f32[8,32,199]{2,1,0:T(8,128)} %broadcast_in_dim.26), calls=%async_computation.4 | async-start | bytes 524288 | tf_op jit(solution)/shard_map/all_to_all | solution.py:18
  67.0 1.2 copy.148
  69.5 2.6 all-to-all-done.4
  72.8 1.1 copy.145
  74.9 1.4 slice.51
  77.0 1.6 slice.48
  78.6 1.1 slice.42
  82.7 1.4 fusion.4
  85.6 1.2 multiply_convert_fusion
  88.6 1.4 fusion.40
  90.0 1.3 multiply_reduce_fusion.1
  91.3 4.5 %fusion.12 = f32[24,2,256]{2,1,0:T(2,128)S(1)} fusion(bf16[24,256,512]{2,1,0:T(8,128)(2,1)} %param.30, bf16[24,2,512]{2,0,1:T(8,128)(2,1)S(1)} %get-tuple-element.20), kind=kOutput, calls=%fused_computation.38 | convolution fusion | flops 12582912 | bytes 6389760 | tf_op jit(solution)/shard_map/bhc,bpc->bhp/dot_general | solution.py:188
  97.0 1.6 fusion.1
  98.9 1.1 copy.154
  100.9 3.9 %all-to-all-start.5 = ((bf16[32,2,384]{2,1,0:T(2,128)(2,1)}), bf16[32,2,384]{2,1,0:T(2,128)(2,1)S(1)}, u32[]{:S(2)}, u32[]{:S(2)}) async-start(bf16[32,2,384]{2,1,0:T(2,128)(2,1)} %reshape.273), calls=%async_computation.5 | async-start | bytes 98304 | tf_op jit(solution)/shard_map/all_to_all | solution.py:210
  104.9 33.6 %all_gather.3 = f32[32,48,2]{1,2,0:T(2,128)S(1)} all-gather(f32[1,48,2]{1,2,0:T(2,128)S(1)} %pad_maximum_fusion.1), channel_id=1, replica_groups=mesh['kv_0'=8,'kv_1'=4,'tp_0'=4,'tp_1'=2] {'kv_0','kv_1'}, dimensions={0}, use_global_device_ids=true | all-gather | bytes 12672 | tf_op jit(solution)/shard_map/all_gather | solution.py:81
  143.2 6.7 %all-to-all-start.6 = ((bf16[32,2,384]{2,1,0:T(2,128)(2,1)}), bf16[32,2,384]{2,1,0:T(2,128)(2,1)S(1)}, u32[]{:S(2)}, u32[]{:S(2)}) async-start(bf16[32,2,384]{2,1,0:T(2,128)(2,1)} %reshape.277), calls=%async_computation.6 | async-start | bytes 98304 | tf_op jit(solution)/shard_map/all_to_all | solution.py:18
  150.0 8.7 %all-to-all-done.6 = bf16[32,2,384]{2,1,0:T(2,128)(2,1)S(1)} async-done(((bf16[32,2,384]{2,1,0:T(2,128)(2,1)}), bf16[32,2,384]{2,1,0:T(2,128)(2,1)S(1)}, u32[]{:S(2)}, u32[]{:S(2)}) %all-to-all-start.6) | async-done | bytes 49184 | tf_op jit(solution)/shard_map/all_to_all | solution.py:18
  161.0 15.8 %all-to-all-start.7 = ((f32[8,1,24]{2,1,0:T(1,128)}), f32[8,1,24]{2,1,0:T(1,128)S(1)}, u32[]{:S(2)}, u32[]{:S(2)}) async-start(f32[8,1,24]{2,1,0:T(1,128)} %broadcast_in_dim.31), calls=%async_computation.7 | async-start | bytes 8192 | tf_op jit(solution)/shard_map/all_to_all | solution.py:18
  176.9 4.4 %all-to-all-done.7 = f32[8,1,24]{2,1,0:T(1,128)S(1)} async-done(((f32[8,1,24]{2,1,0:T(1,128)}), f32[8,1,24]{2,1,0:T(1,128)S(1)}, u32[]{:S(2)}, u32[]{:S(2)}) %all-to-all-start.7) | async-done | bytes 800 | tf_op jit(solution)/shard_map/all_to_all | solution.py:18
  182.0 3.9 %all-to-all-start.8 = ((bf16[8,24,128]{2,1,0:T(8,128)(2,1)}), bf16[8,24,128]{2,1,0:T(8,128)(2,1)S(1)}, u32[]{:S(2)}, u32[]{:S(2)}) async-start(bf16[8,24,128]{2,1,0:T(8,128)(2,1)} %broadcast_in_dim.32), calls=%async_computation.8 | async-start | bytes 98304 | tf_op jit(solution)/shard_map/all_to_all | solution.py:18
  185.9 4.8 %all-to-all-done.8 = bf16[8,24,128]{2,1,0:T(8,128)(2,1)S(1)} async-done(((bf16[8,24,128]{2,1,0:T(8,128)(2,1)}), bf16[8,24,128]{2,1,0:T(8,128)(2,1)S(1)}, u32[]{:S(2)}, u32[]{:S(2)}) %all-to-all-start.8) | async-done | bytes 49184 | tf_op jit(solution)/shard_map/all_to_all | solution.py:18
  191.6 3.9 %all-to-all-start.9 = ((bf16[32,1,1]{2,1,0:T(2,128)(2,1)}), bf16[32,1,1]{2,1,0:T(2,128)(2,1)S(1)}, u32[]{:S(2)}, u32[]{:S(2)}) async-start(bf16[32,1,1]{2,1,0:T(2,128)(2,1)} %copy.161), calls=%async_computation.9 | async-start | bytes 32768 | tf_op jit(solution)/shard_map/all_to_all | solution.py:95
  195.9 8.3 %all-to-all-done.9 = bf16[32,1,1]{2,1,0:T(2,128)(2,1)S(1)} async-done(((bf16[32,1,1]{2,1,0:T(2,128)(2,1)}), bf16[32,1,1]{2,1,0:T(2,128)(2,1)S(1)}, u32[]{:S(2)}, u32[]{:S(2)}) %all-to-all-start.9) | async-done | bytes 96 | tf_op jit(solution)/shard_map/all_to_all | solution.py:95
  204.8 1.3 broadcast_in_dim.33
  206.0 4.0 %all-to-all-start.10 = ((bf16[32,1,1]{2,1,0:T(2,128)(2,1)}), bf16[32,1,1]{2,1,0:T(2,128)(2,1)S(1)}, u32[]{:S(2)}, u32[]{:S(2)}) async-start(bf16[32,1,1]{2,1,0:T(2,128)(2,1)} %broadcast_in_dim.33), calls=%async_computation.10 | async-start | bytes 32768 | tf_op jit(solution)/shard_map/all_to_all | solution.py:18
  210.5 1.1 reduce.16
  212.3 6.1 %all-to-all-done.10 = bf16[32,1,1]{2,1,0:T(2,128)(2,1)S(1)} async-done(((bf16[32,1,1]{2,1,0:T(2,128)(2,1)}), bf16[32,1,1]{2,1,0:T(2,128)(2,1)S(1)}, u32[]{:S(2)}, u32[]{:S(2)}) %all-to-all-start.10) | async-done | bytes 96 | tf_op jit(solution)/shard_map/all_to_all | solution.py:18
  218.4 3.9 %all-to-all-start.13 = ((bf16[32,2,528]{2,1,0:T(2,128)(2,1)}), bf16[32,2,528]{2,1,0:T(2,128)(2,1)S(1)}, u32[]{:S(2)}, u32[]{:S(2)}) async-start(bf16[32,2,528]{2,1,0:T(2,128)(2,1)} %reshape.279), calls=%async_computation.13 | async-start | bytes 163840 | tf_op jit(solution)/shard_map/all_to_all | solution.py:95
  222.6 1.1 reduce.18
  224.5 6.8 %all-to-all-done.13 = bf16[32,2,528]{2,1,0:T(2,128)(2,1)S(1)} async-done(((bf16[32,2,528]{2,1,0:T(2,128)(2,1)}), bf16[32,2,528]{2,1,0:T(2,128)(2,1)S(1)}, u32[]{:S(2)}, u32[]{:S(2)}) %all-to-all-start.13) | async-done | bytes 67616 | tf_op jit(solution)/shard_map/all_to_all | solution.py:95
  231.3 3.9 %all-to-all-start.11 = ((bf16[32,2,528]{2,1,0:T(2,128)(2,1)}), bf16[32,2,528]{2,1,0:T(2,128)(2,1)S(1)}, u32[]{:S(2)}, u32[]{:S(2)}) async-start(bf16[32,2,528]{2,1,0:T(2,128)(2,1)} %reshape.283), calls=%async_computation.11 | async-start | bytes 163840 | tf_op jit(solution)/shard_map/all_to_all | solution.py:95
  235.5 1.1 reduce.17
  237.4 6.8 %all-to-all-done.11 = bf16[32,2,528]{2,1,0:T(2,128)(2,1)S(1)} async-done(((bf16[32,2,528]{2,1,0:T(2,128)(2,1)}), bf16[32,2,528]{2,1,0:T(2,128)(2,1)S(1)}, u32[]{:S(2)}, u32[]{:S(2)}) %all-to-all-start.11) | async-done | bytes 67616 | tf_op jit(solution)/shard_map/all_to_all | solution.py:95
  244.1 3.9 %all-to-all-start.14 = ((bf16[32,2,528]{2,1,0:T(2,128)(2,1)}), bf16[32,2,528]{2,1,0:T(2,128)(2,1)S(1)}, u32[]{:S(2)}, u32[]{:S(2)}) async-start(bf16[32,2,528]{2,1,0:T(2,128)(2,1)} %reshape.281), calls=%async_computation.14 | async-start | bytes 163840 | tf_op jit(solution)/shard_map/all_to_all | solution.py:18
  248.5 1.1 reduce.19
  250.3 6.6 %all-to-all-done.14 = bf16[32,2,528]{2,1,0:T(2,128)(2,1)S(1)} async-done(((bf16[32,2,528]{2,1,0:T(2,128)(2,1)}), bf16[32,2,528]{2,1,0:T(2,128)(2,1)S(1)}, u32[]{:S(2)}, u32[]{:S(2)}) %all-to-all-start.14) | async-done | bytes 67616 | tf_op jit(solution)/shard_map/all_to_all | solution.py:18
  257.0 3.9 %all-to-all-start.12 = ((bf16[32,2,528]{2,1,0:T(2,128)(2,1)}), bf16[32,2,528]{2,1,0:T(2,128)(2,1)S(1)}, u32[]{:S(2)}, u32[]{:S(2)}) async-start(bf16[32,2,528]{2,1,0:T(2,128)(2,1)} %reshape.285), calls=%async_computation.12 | async-start | bytes 163840 | tf_op jit(solution)/shard_map/all_to_all | solution.py:18
  261.5 8.3 %all-to-all-done.12 = bf16[32,2,528]{2,1,0:T(2,128)(2,1)S(1)} async-done(((bf16[32,2,528]{2,1,0:T(2,128)(2,1)}), bf16[32,2,528]{2,1,0:T(2,128)(2,1)S(1)}, u32[]{:S(2)}, u32[]{:S(2)}) %all-to-all-start.12) | async-done | bytes 67616 | tf_op jit(solution)/shard_map/all_to_all | solution.py:18
  271.7 10.9 %all-to-all-start.15 = ((bf16[8,2,192]{2,1,0:T(2,128)(2,1)}), bf16[8,2,192]{2,1,0:T(2,128)(2,1)S(1)}, u32[]{:S(2)}, u32[]{:S(2)}) async-start(bf16[8,2,192]{2,1,0:T(2,128)(2,1)} %reshape.287), calls=%async_computation.15 | async-start | bytes 16384 | tf_op jit(solution)/shard_map/all_to_all | solution.py:95
  282.6 4.6 %all-to-all-done.15 = bf16[8,2,192]{2,1,0:T(2,128)(2,1)S(1)} async-done(((bf16[8,2,192]{2,1,0:T(2,128)(2,1)}), bf16[8,2,192]{2,1,0:T(2,128)(2,1)S(1)}, u32[]{:S(2)}, u32[]{:S(2)}) %all-to-all-start.15) | async-done | bytes 6176 | tf_op jit(solution)/shard_map/all_to_all | solution.py:95
  (140 shorter events, 38.0 us)
Async XLA Ops:
  0.0 96.7 %copy-start = (bf16[24,256,64]{1,2,0:T(8,128)(2,1)S(1)}, bf16[24,256,64]{1,2,0:T(8,128)(2,1)}, u32[]{:S(2)}) copy-start(bf16[24,256,64]{1,2,0:T(8,128)(2,1)} %param.31) | copy-start | bytes 2359300
  0.0 82.7 %copy-start.7 = (f32[1536]{0:T(1024)S(1)}, f32[1536]{0:T(1024)}, u32[]{:S(2)}) copy-start(f32[1536]{0:T(1024)} %param.24) | copy-start | bytes 18436
  37.0 12.5 %all-to-all-start.3 = ((f32[32,1,199]{2,1,0:T(1,128)}), f32[32,1,199]{2,1,0:T(1,128)S(1)}, u32[]{:S(2)}, u32[]{:S(2)}) async-start(f32[32,1,199]{2,1,0:T(1,128)} %broadcast_in_dim.25), calls=%async_computation.3 | async-start | bytes 65536 | tf_op jit(solution)/shard_map/all_to_all | solution.py:18
  49.5 11.4 %all-to-all-start = ((bf16[8,2,192]{2,1,0:T(2,128)(2,1)}), bf16[8,2,192]{2,1,0:T(2,128)(2,1)S(1)}, u32[]{:S(2)}, u32[]{:S(2)}) async-start(bf16[8,2,192]{2,1,0:T(2,128)(2,1)} %reshape.275), calls=%async_computation | async-start | bytes 16384 | tf_op jit(solution)/shard_map/all_to_all | solution.py:18
  61.6 10.5 %all-to-all-start.4 = ((f32[8,32,199]{2,1,0:T(8,128)}), f32[8,32,199]{2,1,0:T(8,128)S(1)}, u32[]{:S(2)}, u32[]{:S(2)}) async-start(f32[8,32,199]{2,1,0:T(8,128)} %broadcast_in_dim.26), calls=%async_computation.4 | async-start | bytes 524288 | tf_op jit(solution)/shard_map/all_to_all | solution.py:18
  66.3 30.6 %slice-start = ((s8[6291456]{0:T(1024)(128)(4,1)}), s8[2097152]{0:T(1024)(128)(4,1)S(1)}, s32[]{:S(2)}) async-start(s8[6291456]{0:T(1024)(128)(4,1)} %bitcast.96), calls=%async_computation.16 | async-start | bytes 4194304
  72.1 0.7 copy-start.1
  90.0 7.0 %slice-start.1 = ((s8[6291456]{0:T(1024)(128)(4,1)}), s8[4194304]{0:T(1024)(128)(4,1)S(1)}, s32[]{:S(2)}) async-start(s8[6291456]{0:T(1024)(128)(4,1)} %bitcast.96), calls=%async_computation.17 | async-start | bytes 8388608
  95.8 54.1 %copy-start.4 = (bf16[8,16,24]{2,1,0:T(8,128)(2,1)S(1)}, bf16[8,16,24]{2,1,0:T(8,128)(2,1)}, u32[]{:S(2)}) copy-start(bf16[8,16,24]{2,1,0:T(8,128)(2,1)} %reshape.276) | copy-start | bytes 18436
  97.0 63.2 %copy-start.5 = (bf16[2,512,128]{2,1,0:T(8,128)(2,1)S(1)}, bf16[2,512,128]{2,1,0:T(8,128)(2,1)}, u32[]{:S(2)}) copy-start(bf16[2,512,128]{2,1,0:T(8,128)(2,1)} %param.29) | copy-start | bytes 786436
  97.0 98.5 %copy-start.2 = (bf16[128,1408]{1,0:T(8,128)(2,1)S(1)}, bf16[128,1408]{1,0:T(8,128)(2,1)}, u32[]{:S(2)}) copy-start(bf16[128,1408]{1,0:T(8,128)(2,1)} %param.36) | copy-start | bytes 1081348
  98.6 78.2 %copy-start.6 = (bf16[256,128]{1,0:T(8,128)(2,1)S(1)}, bf16[256,128]{1,0:T(8,128)(2,1)}, u32[]{:S(2)}) copy-start(bf16[256,128]{1,0:T(8,128)(2,1)} %param.33) | copy-start | bytes 196612
  98.6 78.2 %copy-start.9 = (f32[256]{0:T(256)S(1)}, f32[256]{0:T(256)}, u32[]{:S(2)}) copy-start(f32[256]{0:T(256)} %param.32) | copy-start | bytes 3076
  98.6 96.9 %copy-start.8 = (f32[128]{0:T(128)S(1)}, f32[128]{0:T(128)}, u32[]{:S(2)}) copy-start(f32[128]{0:T(128)} %param.34) | copy-start | bytes 1540
  98.6 123.7 %copy-start.3 = (bf16[128,1408]{1,0:T(8,128)(2,1)S(1)}, bf16[128,1408]{1,0:T(8,128)(2,1)}, u32[]{:S(2)}) copy-start(bf16[128,1408]{1,0:T(8,128)(2,1)} %param.35) | copy-start | bytes 1081348
  100.9 40.0 %all-to-all-start.5 = ((bf16[32,2,384]{2,1,0:T(2,128)(2,1)}), bf16[32,2,384]{2,1,0:T(2,128)(2,1)S(1)}, u32[]{:S(2)}, u32[]{:S(2)}) async-start(bf16[32,2,384]{2,1,0:T(2,128)(2,1)} %reshape.273), calls=%async_computation.5 | async-start | bytes 98304 | tf_op jit(solution)/shard_map/all_to_all | solution.py:210
  138.5 132.1 %copy-start.10 = (bf16[1408,128]{1,0:T(8,128)(2,1)S(1)}, bf16[1408,128]{1,0:T(8,128)(2,1)}, u32[]{:S(2)}) copy-start(bf16[1408,128]{1,0:T(8,128)(2,1)} %param.37) | copy-start | bytes 1081348
  143.2 15.5 %all-to-all-start.6 = ((bf16[32,2,384]{2,1,0:T(2,128)(2,1)}), bf16[32,2,384]{2,1,0:T(2,128)(2,1)S(1)}, u32[]{:S(2)}, u32[]{:S(2)}) async-start(bf16[32,2,384]{2,1,0:T(2,128)(2,1)} %reshape.277), calls=%async_computation.6 | async-start | bytes 98304 | tf_op jit(solution)/shard_map/all_to_all | solution.py:18
  161.0 20.3 %all-to-all-start.7 = ((f32[8,1,24]{2,1,0:T(1,128)}), f32[8,1,24]{2,1,0:T(1,128)S(1)}, u32[]{:S(2)}, u32[]{:S(2)}) async-start(f32[8,1,24]{2,1,0:T(1,128)} %broadcast_in_dim.31), calls=%async_computation.7 | async-start | bytes 8192 | tf_op jit(solution)/shard_map/all_to_all | solution.py:18
  182.0 8.7 %all-to-all-start.8 = ((bf16[8,24,128]{2,1,0:T(8,128)(2,1)}), bf16[8,24,128]{2,1,0:T(8,128)(2,1)S(1)}, u32[]{:S(2)}, u32[]{:S(2)}) async-start(bf16[8,24,128]{2,1,0:T(8,128)(2,1)} %broadcast_in_dim.32), calls=%async_computation.8 | async-start | bytes 98304 | tf_op jit(solution)/shard_map/all_to_all | solution.py:18
  191.6 12.5 %all-to-all-start.9 = ((bf16[32,1,1]{2,1,0:T(2,128)(2,1)}), bf16[32,1,1]{2,1,0:T(2,128)(2,1)S(1)}, u32[]{:S(2)}, u32[]{:S(2)}) async-start(bf16[32,1,1]{2,1,0:T(2,128)(2,1)} %copy.161), calls=%async_computation.9 | async-start | bytes 32768 | tf_op jit(solution)/shard_map/all_to_all | solution.py:95
  206.0 12.4 %all-to-all-start.10 = ((bf16[32,1,1]{2,1,0:T(2,128)(2,1)}), bf16[32,1,1]{2,1,0:T(2,128)(2,1)S(1)}, u32[]{:S(2)}, u32[]{:S(2)}) async-start(bf16[32,1,1]{2,1,0:T(2,128)(2,1)} %broadcast_in_dim.33), calls=%async_computation.10 | async-start | bytes 32768 | tf_op jit(solution)/shard_map/all_to_all | solution.py:18
  218.4 12.9 %all-to-all-start.13 = ((bf16[32,2,528]{2,1,0:T(2,128)(2,1)}), bf16[32,2,528]{2,1,0:T(2,128)(2,1)S(1)}, u32[]{:S(2)}, u32[]{:S(2)}) async-start(bf16[32,2,528]{2,1,0:T(2,128)(2,1)} %reshape.279), calls=%async_computation.13 | async-start | bytes 163840 | tf_op jit(solution)/shard_map/all_to_all | solution.py:95
  231.3 12.8 %all-to-all-start.11 = ((bf16[32,2,528]{2,1,0:T(2,128)(2,1)}), bf16[32,2,528]{2,1,0:T(2,128)(2,1)S(1)}, u32[]{:S(2)}, u32[]{:S(2)}) async-start(bf16[32,2,528]{2,1,0:T(2,128)(2,1)} %reshape.283), calls=%async_computation.11 | async-start | bytes 163840 | tf_op jit(solution)/shard_map/all_to_all | solution.py:95
  244.1 12.8 %all-to-all-start.14 = ((bf16[32,2,528]{2,1,0:T(2,128)(2,1)}), bf16[32,2,528]{2,1,0:T(2,128)(2,1)S(1)}, u32[]{:S(2)}, u32[]{:S(2)}) async-start(bf16[32,2,528]{2,1,0:T(2,128)(2,1)} %reshape.281), calls=%async_computation.14 | async-start | bytes 163840 | tf_op jit(solution)/shard_map/all_to_all | solution.py:18
  257.0 12.8 %all-to-all-start.12 = ((bf16[32,2,528]{2,1,0:T(2,128)(2,1)}), bf16[32,2,528]{2,1,0:T(2,128)(2,1)S(1)}, u32[]{:S(2)}, u32[]{:S(2)}) async-start(bf16[32,2,528]{2,1,0:T(2,128)(2,1)} %reshape.285), calls=%async_computation.12 | async-start | bytes 163840 | tf_op jit(solution)/shard_map/all_to_all | solution.py:18
  271.7 15.5 %all-to-all-start.15 = ((bf16[8,2,192]{2,1,0:T(2,128)(2,1)}), bf16[8,2,192]{2,1,0:T(2,128)(2,1)S(1)}, u32[]{:S(2)}, u32[]{:S(2)}) async-start(bf16[8,2,192]{2,1,0:T(2,128)(2,1)} %reshape.287), calls=%async_computation.15 | async-start | bytes 16384 | tf_op jit(solution)/shard_map/all_to_all | solution.py:95
where the time goes:
time: 290 us; the launch traced here: 288 us
  waiting for transfers between devices  79.8 us (28%)
  starting transfers between devices  79 us (27%)
  blocking collectives  65.4 us (23%)
  local copies, waits for them, and re-layouts  32.7 us (11%)
  other arithmetic  17.4 us (6%)
  matrix products  13.4 us (5%)
    all_to_all x9, waiting for transfers between devices, copy_for_each(): return lax.all_to_all(copies, axis, split_axis=0, concat_axis=0, tiled=True)  53.3 us
    all_to_all x9, starting transfers between devices, copy_for_each(): return lax.all_to_all(copies, axis, split_axis=0, concat_axis=0, tiled=True)  52.7 us
    all_gather x1, blocking collectives, side_by_side(): whole = lax.all_gather(both, axis, axis=dim, tiled=True)  33.6 us
    all_to_all x4, waiting for transfers between devices, sum_at_owner(): lax.all_to_all(parts, axis, split_axis=0, concat_axis=0, tiled=True)  26.5 us
    all_to_all x4, starting transfers between devices, sum_at_owner(): lax.all_to_all(parts, axis, split_axis=0, concat_axis=0, tiled=True)  22.4 us
    all_to_all x1, blocking collectives, sum_in_two_steps(): lax.all_to_all(nearer, far, split_axis=0, concat_axis=0, tiled=True)  19.7 us
    all_to_all x1, blocking collectives, sent_and_summed(): parts = lax.all_to_all(cut_along(x, dim, count), axis, 0, 0, tiled=True)  12.1 us
    unnamed x49, local copies, waits for them, and re-layouts  11.4 us
  transfers between devices with their start and end apart: 14, of which 13 were waited for; matrix products, arithmetic and copies ran while one was open for 6% of the time, Pallas kernels for 0%

commit v1 on v0

v1 whole, which is shorter than its diff:
```python
import functools
import math

import jax
import jax.numpy as jnp
import numpy as np
from jax import lax
from jax.experimental import pallas as pl
from jax.experimental.pallas import tpu as pltpu
from jax.sharding import Mesh
from jax.sharding import PartitionSpec as P

KV, TP = ("z", "yh", "yl"), ("x", "c")
NEAR, FAR = ("yl", "x", "c"), ("z", "yh")
EPS = 1e-06
BASE = 10000.0
MIB = 1 << 20
F32, BF16 = jnp.float32, jnp.bfloat16
NT = (((1,), (1,)), ((), ()))


def mm(a, b):
    return jnp.dot(a, b, preferred_element_type=F32)


def mm_nt(a, b):
    return lax.dot_general(a, b, NT, preferred_element_type=F32)


def diagonal(rows, lanes):
    r = lax.broadcasted_iota(jnp.int32, (rows, lanes), 0)
    return r == lax.broadcasted_iota(jnp.int32, (rows, lanes), 1)


def as_row(col, lanes=128):
    return jnp.sum(jnp.where(diagonal(col.shape[0], lanes), col, 0.0), axis=0, keepdims=True)


def as_col(row, n):
    return jnp.sum(jnp.where(diagonal(n, row.shape[1]), row, 0.0), axis=1, keepdims=True)


def parts_of(x, count):
    out = []
    for _ in range(count):
        top = x.astype(BF16).astype(F32)
        out.append(top)
        x = x - top
    return out


def stacked(rows, lanes=128):
    index = lax.broadcasted_iota(jnp.int32, (8, lanes), 0)
    tile = jnp.zeros((8, lanes), F32)
    for k, row in enumerate(rows):
        tile = jnp.where(index == k, row, tile)
    return tile


def call(body, out, ins, scratch=(), mib=8, flops=1000000, hbm=()):
    single = not isinstance(out, list)
    outs = [out] if single else list(out)
    ins = [pltpu.with_memory_space_constraint(x, pltpu.HBM) if k in hbm else x for k, x in enumerate(ins)]
    got = pl.pallas_call(
        body,
        out_shape=[pltpu.VMEM(s, d) if hbm else jax.ShapeDtypeStruct(s, d) for s, d in outs],
        in_specs=[pl.BlockSpec(memory_space=pltpu.HBM if k in hbm else pltpu.VMEM) for k in range(len(ins))],
        out_specs=[pl.BlockSpec(memory_space=pltpu.VMEM)] * len(outs),
        scratch_shapes=list(scratch),
        compiler_params=pltpu.CompilerParams(vmem_limit_bytes=mib * MIB),
        cost_estimate=pl.CostEstimate(flops=flops, bytes_accessed=100000, transcendentals=0),
    )(*ins)
    return got[0] if single else got


def compress(
    rows, stream_hbm, gain_hbm, query_hbm, latent_hbm, rotary_hbm,
    out_ref, stream_ref, gain_ref, query_ref, latent_ref, rotary_ref, sems,
):
    copies = [
        pltpu.make_async_copy(a, b, sems.at[k])
        for k, (a, b) in enumerate((
            (stream_hbm, stream_ref), (gain_hbm, gain_ref), (rotary_hbm, rotary_ref),
            (latent_hbm, latent_ref), (query_hbm, query_ref),
        ))
    ]
    for copy in copies:
        copy.start()
    for copy in copies:
        copy.wait()
    own_f = mm_nt(diagonal(rows, rows).astype(BF16), stream_ref[...])
    own = own_f.astype(BF16)
    scaled = (own_f * gain_ref[...]).astype(BF16)
    query = mm(scaled, query_ref[...])
    latent = mm(scaled, latent_ref[...])
    rotary = mm(scaled, rotary_ref[...]).astype(BF16)
    wide = rotary.shape[1]
    turned = mm_nt(diagonal(wide, wide).astype(BF16), rotary)
    square = jnp.broadcast_to(as_row(jnp.sum(own_f * own_f, axis=1, keepdims=True)), (8, 128)).astype(BF16)
    count = own.shape[1]
    chunks = out_ref.shape[0]
    piece = wide // chunks
    for j in range(chunks):
        at = 128 * j
        part = query[:, at : at + 128] if at < query.shape[1] else latent[:, at - query.shape[1] : at - query.shape[1] + 128]
        out_ref[j, :rows, :] = part.astype(BF16)
        out_ref[j, rows:, :] = square
        out_ref[j, rows : rows + piece, :rows] = turned[piece * j : piece * (j + 1), :].astype(BF16)
        for g in range(rows // 8):
            out_ref[j, rows:, 32 + count * g : 32 + count * (g + 1)] = own[8 * g : 8 * g + 8, :]


def total_of(in_ref):
    total = in_ref[0].astype(F32)
    for p in range(1, in_ref.shape[0]):
        total += in_ref[p].astype(F32)
    return total


def first_sum(rows, count, in_ref, out_ref, block_ref):
    total = total_of(in_ref).astype(BF16)
    for k in range(out_ref.shape[0]):
        out_ref[k] = total
    peers = block_ref.shape[1] // count
    base = peers * lax.axis_index("yl")
    for p in range(peers):
        for g in range(rows // 8):
            block_ref[8 * g : 8 * g + 8, count * p : count * (p + 1)] = in_ref[base + p, rows:, 32 + count * g : 32 + count * (g + 1)]


def plain_sum(in_ref, out_ref):
    total = total_of(in_ref).astype(BF16)
    for k in range(out_ref.shape[0]):
        out_ref[k] = total


def fetch(count, token_ref, *refs):
    sources, targets, sems = refs[:count], refs[count:-1], refs[-1]
    copies = [pltpu.make_async_copy(a, b, sems.at[k]) for k, (a, b) in enumerate(zip(sources, targets))]
    for copy in copies:
        copy.start()
    for copy in copies:
        copy.wait()


def attend(
    rows, width, scale,
    in_ref, qgain_ref, lgain_ref, trig_ref,
    content_ref, rotary_ref, key_ref, value_ref, turned_ref, latents_hbm,
    out_ref, q_ref, qt_ref, s_ref, w_ref, r_ref, latents_ref, sems,
):
    group = rows // sems.shape[0]
    copies = [
        pltpu.make_async_copy(latents_hbm.at[group * k : group * (k + 1)], latents_ref.at[group * k : group * (k + 1)], sems.at[k])
        for k in range(sems.shape[0])
    ]
    for copy in copies:
        copy.start()
    heads = key_ref.shape[0]
    extent = turned_ref.shape[1]
    half = extent // 2
    pieces = q_ref.shape[0]
    chunks = in_ref.shape[0]
    n_query = qgain_ref.shape[0]
    eye = diagonal(rows, 128)
    part = extent // chunks
    first_row = lax.rsqrt(in_ref[0, rows + part : rows + part + 1, :].astype(F32) / width + EPS)
    first = as_col(first_row, rows)

    def normed_of(tiles, gain_ref):
        tiles = [in_ref[j, :rows, :].astype(F32) * first for j in tiles]
        square = jnp.sum(sum(x * x for x in tiles), axis=1, keepdims=True)
        inverse = lax.rsqrt(square / (128 * len(tiles)) + EPS)
        return jnp.concatenate([x * inverse * gain_ref[j : j + 1, :] for j, x in enumerate(tiles)], axis=1).astype(BF16)

    normed = normed_of(range(n_query), qgain_ref)
    row = normed_of(range(n_query, chunks), lgain_ref).astype(F32)
    for j in range(chunks):
        r_ref[part * j : part * (j + 1), :] = in_ref[j, rows : rows + part, :].astype(F32) * first_row
    low_half, high_half = r_ref[:half, :], r_ref[half:extent, :]
    cos_t, sin_t = trig_ref[:half, :], trig_ref[half : 2 * half, :]
    spun = jnp.concatenate([low_half * cos_t - high_half * sin_t, high_half * cos_t + low_half * sin_t], axis=0).astype(BF16)

    plain = mm(normed, content_ref[...]).astype(BF16)
    turn = mm(normed, rotary_ref[...])
    lane = lax.broadcasted_iota(jnp.int32, turn.shape, 1)
    across = turn.shape[1]
    swapped = jnp.where(lane % extent < half, pltpu.roll(turn, across - half, 1), pltpu.roll(turn, half, 1))
    turn = (turn * trig_ref[2 * half : 2 * half + 1, :] + swapped * trig_ref[2 * half + 1 : 2 * half + 2, :]).astype(BF16)
    turn_f = turn.astype(F32)

    q_ref[...] = jnp.zeros_like(q_ref)
    qt_ref[...] = jnp.zeros_like(qt_ref)
    own = []
    for h in range(heads):
        absorbed = mm(plain[:, 128 * h : 128 * h + 128], key_ref[h]).astype(BF16).astype(F32)
        for c in range(pieces):
            q_ref[c, pl.ds(h, rows, 8), :] = absorbed[:, 128 * c : 128 * c + 128]
        qt_ref[pl.ds(h, rows, 8), :] = turn_f if h == 0 else pltpu.roll(turn_f, across - extent * h, 1)
        turned_h = turn[:, extent * h : extent * (h + 1)]
        cross = jnp.sum(jnp.where(eye, mm(turned_h, spun), 0.0), axis=1, keepdims=True)
        own.append((jnp.sum(absorbed * row, axis=1, keepdims=True) + cross) * scale)

    for b in range(rows):
        if b % group == 0:
            copies[b // group].wait()
        at = slice(8 * b, 8 * b + 8)
        asked = jnp.concatenate([q_ref[c, at, :] for c in range(pieces)], axis=1).astype(BF16)
        s_ref[at, :] = (mm_nt(asked, latents_ref[b]) + mm(qt_ref[at, :extent].astype(BF16), turned_ref[b])) * scale
    scores = s_ref[...]
    tops = jnp.max(scores, axis=1, keepdims=True)
    expo = jnp.exp(scores - tops)
    s_ref[...] = expo
    r_ref[: 8 * rows, :] = jnp.broadcast_to(tops, (8 * rows, 128))
    r_ref[8 * rows :, :] = jnp.broadcast_to(jnp.sum(expo, axis=1, keepdims=True), (8 * rows, 128))
    for b in range(rows):
        at = slice(8 * b, 8 * b + 8)
        weighted = mm(s_ref[at, :].astype(BF16), latents_ref[b])
        for c in range(pieces):
            w_ref[c, at, :] = weighted[:, 128 * c : 128 * c + 128]

    here = lax.axis_index(KV) == 0
    values, logs = [], []
    for h in range(heads):
        weighted = jnp.concatenate([w_ref[c, pl.ds(h, rows, 8), :] for c in range(pieces)], axis=1)
        top = r_ref[pl.ds(h, rows, 8), :][:, :1]
        total = r_ref[pl.ds(8 * rows + h, rows, 8), :][:, :1]
        mine = jnp.where(here, own[h], -1e30)
        peak = jnp.maximum(top, mine)
        keep = jnp.exp(top - peak)
        add = jnp.exp(mine - peak)
        total = total * keep + add
        mixed = ((weighted * keep + row * add) / total).astype(BF16)
        values.append(mm(mixed, value_ref[h]).astype(BF16))
        logs += parts_of(as_row(peak + jnp.log(total)), 3)
    tile = stacked(logs).astype(BF16)
    for k in range(out_ref.shape[0]):
        for h in range(heads):
            out_ref[k, rows * h : rows * (h + 1), :] = values[h]
        out_ref[k, rows * heads :, :] = tile


def project(rows, in_ref, gain_ref, weight_ref, out_ref):
    blocks = in_ref.shape[0]
    heads = in_ref.shape[1] // rows
    logs = []
    for k in range(blocks):
        tile = in_ref[k, rows * heads :, :].astype(F32)
        logs.append(tile + pltpu.roll(tile, 7, 0) + pltpu.roll(tile, 6, 0))
    peak = functools.reduce(jnp.maximum, logs)
    factors = [jnp.exp(x - peak) for x in logs]
    whole = 1.0 / functools.reduce(jnp.add, factors)
    spread = jnp.concatenate([x * whole for x in factors], axis=0)
    eye = diagonal(rows, 128).astype(BF16)
    columns = sum(mm_nt(eye, x.astype(BF16)) for x in parts_of(spread, 2))
    values = []
    for h in range(heads):
        total = jnp.zeros((rows, 128), F32)
        for k in range(blocks):
            total += columns[:, 8 * k + 3 * h : 8 * k + 3 * h + 1] * in_ref[k, rows * h : rows * (h + 1), :].astype(F32)
        values.append(total.astype(BF16).astype(F32))
    values = jnp.concatenate(values, axis=1)
    square = as_row(jnp.sum(values * values, axis=1, keepdims=True))
    scaled = (values * gain_ref[...]).astype(BF16)
    product = mm(scaled, weight_ref[...]).astype(BF16)
    tile = stacked(parts_of(square, 2)).astype(BF16)
    for p in range(out_ref.shape[0]):
        out_ref[p, :rows, :] = product
        out_ref[p, rows:, :] = tile


def spots(rows, tiles):
    return [(8 * (t // tiles), 128 * (t % tiles)) for t in range(rows // 8 * tiles)]


def expand(rows, width, in_ref, block_ref, gain_ref, gate_ref, up_ref, out_ref, middle_ref):
    attended = total_of(in_ref)
    head_row = lax.rsqrt((attended[rows : rows + 1] + attended[rows + 1 : rows + 2]) / width + EPS)
    middle = (block_ref[...].astype(F32) + as_col(head_row, rows) * attended[:rows]).astype(BF16)
    middle_ref[...] = middle
    middle = middle.astype(F32)
    square = as_row(jnp.sum(middle * middle, axis=1, keepdims=True))
    tile = stacked(parts_of(square, 2)).astype(BF16)
    scaled = (middle * gain_ref[...]).astype(BF16)
    places = spots(rows, gate_ref.shape[1] // 128)
    owners = out_ref.shape[0]
    spare = len(places) - owners
    for at, weight_ref in ((0, gate_ref), (8, up_ref)):
        product = mm(scaled, weight_ref[...])
        for t in range(owners):
            for slot, (r, c) in enumerate([places[t]] + places[owners:]):
                out_ref[t, 16 * slot + at : 16 * slot + at + 8, :] = product[r : r + 8, c : c + 128].astype(BF16)
    for t in range(owners):
        out_ref[t, 16 * (1 + spare) :, :] = tile


def activate(rows, width, tiles, in_ref, out_ref, rest_ref, scale_ref):
    total = total_of(in_ref)
    owners = out_ref.shape[0]
    places = spots(rows, tiles)
    spare = len(places) - owners
    last = 16 * (1 + spare)
    scale_row = lax.rsqrt((total[last : last + 1] + total[last + 1 : last + 2]) / width + EPS)
    scale_ref[...] = jnp.broadcast_to(as_col(scale_row, rows), scale_ref.shape)

    def hidden(slot, scale):
        gate = total[16 * slot : 16 * slot + 8] * scale
        up = total[16 * slot + 8 : 16 * slot + 16] * scale
        return (gate / (1.0 + jnp.exp(-gate)) * up).astype(BF16)

    group = lax.axis_index(KV) // tiles
    mine = hidden(0, scale_ref[pl.ds(pl.multiple_of(8 * group, 8), 8), :])
    for k in range(owners):
        out_ref[k] = mine
    for s in range(spare):
        r, _ = places[owners + s]
        rest_ref[8 * s : 8 * s + 8, :] = hidden(1 + s, scale_ref[r : r + 8, :])


def contract(rows, tiles, in_ref, rest_ref, weight_ref, out_ref, hidden_ref):
    owners = in_ref.shape[0]
    for t, (r, c) in enumerate(spots(rows, tiles)):
        part = in_ref[t] if t < owners else rest_ref[8 * (t - owners) : 8 * (t - owners) + 8, :]
        hidden_ref[r : r + 8, c : c + 128] = part
    product = mm(hidden_ref[...], weight_ref[...]).astype(BF16)
    for p in range(out_ref.shape[0]):
        out_ref[p] = product


def finish(in_ref, middle_ref, out_ref):
    total = (middle_ref[...].astype(F32) + total_of(in_ref)).astype(BF16)
    width = out_ref.shape[0]
    at = (width, total.shape[1])
    row = lax.broadcasted_iota(jnp.int32, at, 0) + width * lax.axis_index(TP)
    pick = (row == lax.broadcasted_iota(jnp.int32, at, 1)).astype(BF16)
    out_ref[...] = mm_nt(pick, total).astype(BF16)


def exchange(x, axis):
    return lax.all_to_all(x, axis, 0, 0, tiled=True)


def local(
    stream, attention_gain, query_down, latent_down, rotary_down, query_gain, latent_gain,
    query_content, query_rotary, key_absorb, value_absorb, latent_cache, rotary_cache,
    head_gain, output_weight, mixer_gain, gate_weight, up_weight, down_weight,
):
    kv, tp = lax.axis_size(KV), lax.axis_size(TP)
    near, far = lax.axis_size(NEAR), lax.axis_size(FAR)
    rows, count = stream.shape
    width = count * kv * tp
    heads, nope, latent = key_absorb.shape
    rope = rotary_cache.shape[2]
    block_len = latent_cache.shape[1]
    position = block_len * kv
    scale = (nope + rope) ** (-0.5)
    tiles = gate_weight.shape[1] // 128
    spare = rows // 8 * tiles - kv
    angle = position * BASE ** (-np.arange(rope // 2) * 2.0 / rope)
    cos, sin = np.cos(angle), np.sin(angle)
    trig = np.concatenate([
        np.tile(cos[:, None], (1, 128)), np.tile(sin[:, None], (1, 128)),
        np.tile(np.concatenate([cos, cos]), heads)[None], np.tile(np.concatenate([-sin, sin]), heads)[None],
        np.zeros((6, 128)),
    ])
    trig = jnp.asarray(trig, F32)
    lines = rows + 8

    sources = (stream.T, attention_gain[None], query_down, latent_down, rotary_down)
    sent = call(
        functools.partial(compress, rows), ((near, lines, 128), BF16), sources,
        scratch=[pltpu.VMEM(x.shape, x.dtype) for x in sources] + [pltpu.SemaphoreType.DMA((len(sources),))],
        hbm=range(len(sources)),
    )
    sent, block = call(
        functools.partial(first_sum, rows, count), [((far, lines, 128), BF16), ((rows, count * tp), BF16)],
        (exchange(sent, NEAR),),
    )
    sources = (
        query_gain.reshape(-1, 128), latent_gain.reshape(-1, 128), trig,
        query_content, query_rotary, key_absorb, value_absorb, jnp.swapaxes(rotary_cache, 1, 2),
    )
    held = call(
        functools.partial(fetch, len(sources)), [(x.shape, x.dtype) for x in sources], (block, *sources),
        scratch=[pltpu.SemaphoreType.DMA((len(sources),))], hbm=range(1, len(sources) + 1), flops=20000000,
    )
    sent = call(plain_sum, ((near, lines, 128), BF16), (exchange(sent, FAR),))
    sent = call(
        functools.partial(attend, rows, width, scale), ((kv, rows * heads + 8, 128), BF16),
        (exchange(sent, NEAR), *held, latent_cache),
        scratch=[
            pltpu.VMEM((latent // 128, 8 * rows, 128), F32), pltpu.VMEM((8 * rows, heads * rope), F32),
            pltpu.VMEM((8 * rows, block_len), F32), pltpu.VMEM((latent // 128, 8 * rows, 128), F32),
            pltpu.VMEM((16 * rows, 128), F32), pltpu.VMEM(latent_cache.shape, BF16), pltpu.SemaphoreType.DMA((4,)),
        ],
        mib=24, hbm=(1 + len(held),),
    )
    sent = call(
        functools.partial(project, rows), ((tp, lines, 128), BF16),
        (exchange(sent, KV), head_gain[None], output_weight),
    )
    sent, middle = call(
        functools.partial(expand, rows, head_gain.shape[0] * tp),
        [((kv, 16 * (1 + spare) + 8, 128), BF16), ((rows, 128), BF16)],
        (exchange(sent, TP), block, mixer_gain[None], gate_weight, up_weight),
    )
    sent, rest = call(
        functools.partial(activate, rows, width, tiles), [((kv, 8, 128), BF16), ((8 * spare, 128), BF16)],
        (exchange(sent, KV),), scratch=[pltpu.VMEM((rows, 128), F32)],
    )
    sent = call(
        functools.partial(contract, rows, tiles), ((tp, rows, 128), BF16),
        (exchange(sent, KV), rest, down_weight), scratch=[pltpu.VMEM((rows, 128 * tiles), BF16)],
    )
    return call(finish, ((count, rows), BF16), (exchange(sent, TP), middle)).T


def solution(mesh):
    grid = Mesh(mesh.devices.reshape(mesh.shape["kv"] // 4, 2, 2, mesh.shape["tp"] // 2, 2), KV + TP)
    both = KV + TP
    return jax.shard_map(
        local,
        mesh=grid,
        in_specs=(
            P(None, both), P(both), P(both, None), P(both, None), P(both, None), P(), P(),
            P(None, TP), P(None, TP), P(TP, None, None), P(TP, None, None),
            P(None, KV, None), P(None, KV, None), P(TP), P(TP, KV), P(KV),
            P(KV, TP), P(KV, TP), P(TP, KV),
        ),
        out_specs=P(None, both),
        check_vma=False,
    )
```

time: 290 us -> 122 us (0.42)
  waiting for transfers between devices: 79.8 us -> 4.22 us
  starting transfers between devices: 79 us -> 5.39 us
  blocking collectives: 65.4 us -> 101 us
  local copies, waits for them, and re-layouts: 32.7 us -> 0.03 us
  other arithmetic: 17.4 us -> 0 us
  matrix products: 13.4 us -> 0 us
  Pallas kernels: 0 us -> 11.3 us
    all_to_all x14 -> x1, waiting for transfers between devices: 79.8 us -> 4.22 us  [exchange(): return lax.all_to_all(x, axis, 0, 0, tiled=True)]
    all_to_all x14 -> x1, starting transfers between devices: 79 us -> 5.39 us  [exchange(): return lax.all_to_all(x, axis, 0, 0, tiled=True)]
    all_to_all x2 -> x7, blocking collectives: 31.8 us -> 101 us  [exchange(): return lax.all_to_all(x, axis, 0, 0, tiled=True)]
    all_gather x1 -> x0, blocking collectives: 33.6 us -> none  [side_by_side(): whole = lax.all_gather(both, axis, axis=dim, tiled=True)]
    dot_general x14 -> x0, matrix products: 13.4 us -> none  [the longest x9 5.38 us: matmul(): return jnp.dot(left, right, preferred_element_type=jnp.float32)]
    pallas_call x0 -> x10, Pallas kernels: none -> 11.3 us  [call(): pl.pallas_call(body, out_shape=[pltpu.VMEM(s, d) if hbm else jax.ShapeDty...]
    unnamed x49 -> x12, local copies, waits for them, and re-layouts: 11.4 us -> 0.03 us
    broadcast_in_dim x8 -> x0, local copies, waits for them, and re-layouts: 5.07 us -> none  [the longest x7 3.98 us: copy_for_each(): copies = jnp.broadcast_to(x, (lax.axis_size(axis), *x.shape))]
  transfers between devices with their start and end apart: 14 -> 1, of which waited for: 13 -> 1; matrix products, arithmetic and copies ran while one was open for 6% -> 0% of each run, Pallas kernels for 0% -> 2%
where the time goes in v1:
time: 122 us
  blocking collectives  101 us (83%)
  Pallas kernels  11.3 us (9%)
  starting transfers between devices  5.39 us (4%)
  waiting for transfers between devices  4.22 us (3%)
    all_to_all x7, blocking collectives, exchange(): return lax.all_to_all(x, axis, 0, 0, tiled=True)  101 us
    pallas_call x10, Pallas kernels, call(): pl.pallas_call(body, out_shape=[pltpu.VMEM(s, d) if hbm else jax.ShapeDty...  11.3 us
    all_to_all x1, starting transfers between devices, exchange(): return lax.all_to_all(x, axis, 0, 0, tiled=True)  5.39 us
    all_to_all x1, waiting for transfers between devices, exchange(): return lax.all_to_all(x, axis, 0, 0, tiled=True)  4.22 us
  transfers between devices with their start and end apart: 1, of which 1 were waited for; matrix products, arithmetic and copies ran while one was open for 0% of the time, Pallas kernels for 2%

profile of v1, /device:TPU:1, one launch (start us, length us, event | category | flops | bytes accessed | tf_op | source)
XLA Modules:
  0.0 121.9 jit_solution(1858299563735340464)
XLA Ops:
  0.0 1.3 %shard_map.190 = bf16[16,32,128]{2,1,0:T(8,128)(2,1)S(1)} custom-call(bf16[16,24]{1,0:T(8,128)(2,1)} %bitcast.12, f32[1,16]{1,0:T(1,128)} %bitcast.14, bf16[16,1536]{1,0:T(8,128)(2,1)} %query_hbm.1, bf16[16,512]{1,0:T(8,128)(2,1)} %latent_hbm.1, bf16[16,64]{1,0:T(8,128)(2,1)} %rotary_hbm.1), custom_call_target="tpu_custom_call" | custom-call | flops 1000000 | bytes 100000 | tf_op jit(solution)/shard_map/pallas_call | solution.py:64
  1.3 12.7 %all_to_all.40.in_ref = bf16[16,32,128]{2,1,0:T(8,128)(2,1)S(1)} all-to-all(bf16[16,32,128]{2,1,0:T(8,128)(2,1)S(1)} %shard_map.190), channel_id=1, replica_groups=mesh['z'=8,'yh'=2,'yl'=2,'x'=4,'c'=2] {'yl','x','c'}, dimensions={0} | all-to-all | bytes 262144 | tf_op jit(solution)/shard_map/all_to_all | solution.py:340
  14.0 0.1 shard_map.191
  14.1 20.4 %all_to_all.41.in_ref = bf16[16,32,128]{2,1,0:T(8,128)(2,1)S(1)} all-to-all(bf16[16,32,128]{2,1,0:T(8,128)(2,1)S(1)} %get-tuple-element.19), channel_id=1, replica_groups=mesh['z'=8,'yh'=2,'yl'=2,'x'=4,'c'=2] {'z','yh'}, dimensions={0} | all-to-all | bytes 262144 | tf_op jit(solution)/shard_map/all_to_all | solution.py:340
  34.5 0.7 shard_map.192
  35.2 5.4 %all-to-all-start.2 = ((bf16[16,32,128]{2,1,0:T(8,128)(2,1)}), bf16[16,32,128]{2,1,0:T(8,128)(2,1)S(1)}, u32[]{:S(2)}, u32[]{:S(2)}) async-start(bf16[16,32,128]{2,1,0:T(8,128)(2,1)} %shard_map.192), calls=%async_computation.2 | async-start | bytes 262144 | tf_op jit(solution)/shard_map/all_to_all | solution.py:340
  40.6 0.0 copy-start.3
  40.6 0.0 copy-start.4
  40.6 0.0 copy-start
  40.6 0.0 copy-start.1
  40.6 0.0 copy-start.5
  40.6 1.8 %shard_map.193 = (f32[12,128]{1,0:T(8,128)S(1)}, f32[4,128]{1,0:T(4,128)S(1)}, f32[72,128]{1,0:T(8,128)S(1)}, bf16[1536,256]{1,0:T(8,128)(2,1)S(1)}, bf16[1536,1...) custom-call(bf16[24,128]{1,0:T(8,128)(2,1)S(1)} %get-tuple-element.2, ...), custom_call_target="tpu_custom_call" | custom-call | flops 20000000 | bytes 100000 | tf_op jit(solution)/shard_map/pallas_call | solution.py:64
  42.5 4.2 %all-to-all-done.2.in_ref = bf16[16,32,128]{2,1,0:T(8,128)(2,1)S(1)} async-done(((bf16[16,32,128]{2,1,0:T(8,128)(2,1)}), bf16[16,32,128]{2,1,0:T(8,128)(2,1)S(1)}, u32[]{:S(2)}, u32[]{:S(2)}) %all-to-all-start.2) | async-done | bytes 131104 | tf_op jit(solution)/shard_map/all_to_all | solution.py:340
  46.7 0.0 copy-start.2
  46.7 5.3 %shard_map.194 = bf16[32,56,128]{2,1,0:T(8,128)(2,1)S(1)} custom-call(bf16[16,32,128]{2,1,0:T(8,128)(2,1)S(1)} %all-to-all-done.2.in_ref, f32[12,128]{1,0:T(8,128)S(1)} %get-tuple-element.21.qgain_ref, f32[4,128]{1,0:T(4,128)S(1)} %get-tuple-element.22.lgain_ref, f32[72,128]{1,0:T(8,128)S(1)} %get-tuple-element.23.trig_ref, ...), custom_call_target="tpu_custom_call" | custom-call | flops 1000000 | bytes 100000 | tf_op jit(solution)/shard_map/pallas_call | solution.py:64
  52.0 18.5 %all_to_all.42.in_ref = bf16[32,56,128]{2,1,0:T(8,128)(2,1)S(1)} all-to-all(bf16[32,56,128]{2,1,0:T(8,128)(2,1)S(1)} %shard_map.194), channel_id=1, replica_groups=mesh['z'=8,'yh'=2,'yl'=2,'x'=4,'c'=2] {'z','yh','yl'}, dimensions={0} | all-to-all | bytes 917504 | tf_op jit(solution)/shard_map/all_to_all | solution.py:340
  70.4 0.0 copy-done.3
  70.4 0.0 copy-done.4
  70.4 0.8 shard_map.195
  71.2 9.2 %all_to_all.43.in_ref = bf16[8,32,128]{2,1,0:T(8,128)(2,1)S(1)} all-to-all(bf16[8,32,128]{2,1,0:T(8,128)(2,1)S(1)} %shard_map.195), channel_id=1, replica_groups=mesh['z'=8,'yh'=2,'yl'=2,'x'=4,'c'=2] {'x','c'}, dimensions={0} | all-to-all | bytes 131072 | tf_op jit(solution)/shard_map/all_to_all | solution.py:340
  80.4 0.0 copy-done
  80.5 0.0 copy-done.1
  80.5 0.0 copy-done.5
  80.5 0.3 shard_map.196
  80.8 16.5 %all_to_all.44.in_ref = bf16[32,40,128]{2,1,0:T(8,128)(2,1)S(1)} all-to-all(bf16[32,40,128]{2,1,0:T(8,128)(2,1)S(1)} %get-tuple-element.29), channel_id=1, replica_groups=mesh['z'=8,'yh'=2,'yl'=2,'x'=4,'c'=2] {'z','yh','yl'}, dimensions={0} | all-to-all | bytes 655360 | tf_op jit(solution)/shard_map/all_to_all | solution.py:340
  97.3 0.1 shard_map.197
  97.4 13.7 %all_to_all.45.in_ref = bf16[32,8,128]{2,1,0:T(8,128)(2,1)S(1)} all-to-all(bf16[32,8,128]{2,1,0:T(8,128)(2,1)S(1)} %get-tuple-element.30), channel_id=1, replica_groups=mesh['z'=8,'yh'=2,'yl'=2,'x'=4,'c'=2] {'z','yh','yl'}, dimensions={0} | all-to-all | bytes 131072 | tf_op jit(solution)/shard_map/all_to_all | solution.py:340
  111.1 0.0 copy-done.2
  111.1 0.2 shard_map.198
  111.3 9.9 %all_to_all.46.in_ref = bf16[8,24,128]{2,1,0:T(8,128)(2,1)S(1)} all-to-all(bf16[8,24,128]{2,1,0:T(8,128)(2,1)S(1)} %shard_map.198), channel_id=1, replica_groups=mesh['z'=8,'yh'=2,'yl'=2,'x'=4,'c'=2] {'x','c'}, dimensions={0} | all-to-all | bytes 98304 | tf_op jit(solution)/shard_map/all_to_all | solution.py:340
  121.2 0.7 shard_map.199
Async XLA Ops:
  35.2 11.5 %all-to-all-start.2 = ((bf16[16,32,128]{2,1,0:T(8,128)(2,1)}), bf16[16,32,128]{2,1,0:T(8,128)(2,1)S(1)}, u32[]{:S(2)}, u32[]{:S(2)}) async-start(bf16[16,32,128]{2,1,0:T(8,128)(2,1)} %shard_map.192), calls=%async_computation.2 | async-start | bytes 262144 | tf_op jit(solution)/shard_map/all_to_all | solution.py:340
  40.6 29.9 %copy-start.3 = (bf16[256,128]{1,0:T(8,128)(2,1)S(1)}, bf16[256,128]{1,0:T(8,128)(2,1)}, u32[]{:S(2)}) copy-start(bf16[256,128]{1,0:T(8,128)(2,1)} %weight_ref.2) | copy-start | bytes 196612
  40.6 29.9 %copy-start.4 = (f32[256]{0:T(256)S(1)}, f32[256]{0:T(256)}, u32[]{:S(2)}) copy-start(f32[256]{0:T(256)} %param.33) | copy-start | bytes 3076
  40.6 39.9 %copy-start = (bf16[128,1408]{1,0:T(8,128)(2,1)S(1)}, bf16[128,1408]{1,0:T(8,128)(2,1)}, u32[]{:S(2)}) copy-start(bf16[128,1408]{1,0:T(8,128)(2,1)} %gate_ref.1) | copy-start | bytes 1081348
  40.6 39.9 %copy-start.1 = (bf16[128,1408]{1,0:T(8,128)(2,1)S(1)}, bf16[128,1408]{1,0:T(8,128)(2,1)}, u32[]{:S(2)}) copy-start(bf16[128,1408]{1,0:T(8,128)(2,1)} %up_ref.1) | copy-start | bytes 1081348
  40.6 39.8 %copy-start.5 = (f32[128]{0:T(128)S(1)}, f32[128]{0:T(128)}, u32[]{:S(2)}) copy-start(f32[128]{0:T(128)} %param.35) | copy-start | bytes 1540
  46.7 64.4 %copy-start.2 = (bf16[1408,128]{1,0:T(8,128)(2,1)S(1)}, bf16[1408,128]{1,0:T(8,128)(2,1)}, u32[]{:S(2)}) copy-start(bf16[1408,128]{1,0:T(8,128)(2,1)} %weight_ref.3) | copy-start | bytes 1081348
